TPU v7x, 32 devices: a whole 2x2x4 slice. The times are simulated.
32 devices in a mesh: rep: 4 (over z), fs: 2 (over y), tp: 4 (over x, core).
Axes of the slice: x: 2, y: 2, z: 4, core: 2. Of those that a mesh axis runs over, the one named last changes fastest.
Arguments:
- tokens: bfloat16 [1536, 2048], P('rep', ('fs', 'tp')), may hold values from -6 to 6
- cotangent: bfloat16 [1536, 2048], P('rep', ('fs', 'tp')), may hold values from -6 to 6
- gain: float32 [2048], replicated, may hold values from 0.1 to 1.9
- w_gate: bfloat16 [5376, 2048], P(('fs', 'tp')), may hold values from -0.125 to 0.125
- w_up: bfloat16 [5376, 2048], P(('fs', 'tp')), may hold values from -0.125 to 0.125
- w_down: bfloat16 [5376, 2048], P(('fs', 'tp')), may hold values from -0.078125 to 0.078125
Outputs:
- grad_input: bfloat16 [1536, 2048], P('rep', ('fs', 'tp'))
- grad_gain: float32 [2048], P(('fs', 'tp'))
- grad_gate: float32 [5376, 2048], P(('fs', 'tp'))
- grad_up: float32 [5376, 2048], P(('fs', 'tp'))
- grad_down: float32 [5376, 2048], P(('fs', 'tp'))
All inputs are finite; a program needn't handle non-finite values.
Results may differ from a plain program's by a relative error of at most 0.006.
Values may be sent and summed in bfloat16 or wider, within the bound.
A program may use at most 128 MiB of HBM per device.

v0:
```python
import jax
import jax.numpy as jnp
from jax import lax
from jax.sharding import PartitionSpec as P

EPS = 1e-06


def right_product(left, weight):
    return lax.dot_general(
        left, weight, (((1,), (1,)), ((), ())), preferred_element_type=jnp.float32
    )


def left_product(left, right):
    return lax.dot_general(
        left, right, (((0,), (0,)), ((), ())), preferred_element_type=jnp.float32
    )


def local(tokens, cotangent, gain, w_gate, w_up, w_down):
    full_x, full_dy = (
        lax.all_gather(tokens, ("fs", "tp"), axis=1, tiled=True),
        lax.all_gather(cotangent, ("fs", "tp"), axis=1, tiled=True),
    )
    xf = full_x.astype(jnp.float32)
    inv_rms = lax.rsqrt(jnp.mean(xf * xf, axis=1, keepdims=True) + EPS)
    unit = xf * inv_rms
    normed = (unit * gain).astype(jnp.bfloat16)
    gate = right_product(normed, w_gate)
    up = right_product(normed, w_up)
    sig = jax.nn.sigmoid(gate)
    active = gate * sig
    hidden = (active * up).astype(jnp.bfloat16)
    d_hidden = 0.5 * right_product(full_dy, w_down)
    d_gate = (d_hidden * up * sig * (1.0 + gate * (1.0 - sig))).astype(jnp.bfloat16)
    d_up = (d_hidden * active).astype(jnp.bfloat16)
    grad_down = 0.5 * left_product(hidden, full_dy)
    grad_gate = left_product(d_gate, normed)
    grad_up = left_product(d_up, normed)
    width = full_x.shape[1]
    partial_value = jnp.dot(d_gate, w_gate, preferred_element_type=jnp.float32) + jnp.dot(
        d_up, w_up, preferred_element_type=jnp.float32
    )
    summed = lax.psum_scatter(partial_value, ("fs", "tp"), scatter_dimension=1, tiled=True)
    own_width = summed.shape[1]
    unit_own = tokens.astype(jnp.float32) * inv_rms
    gain_own = lax.dynamic_slice_in_dim(
        gain, lax.axis_index(("fs", "tp")) * own_width, own_width, 0
    )
    d_unit = summed * gain_own
    row_mean = lax.psum(jnp.sum(unit_own * d_unit, axis=1), ("fs", "tp")) / width
    gain_part = jnp.sum(unit_own * summed, axis=0)
    grad_gate, grad_up, grad_down, grad_gain = lax.psum(
        (grad_gate, grad_up, grad_down, gain_part), "rep"
    )
    grad_input = (
        cotangent.astype(jnp.float32) + inv_rms * (d_unit - unit_own * row_mean[:, None])
    ).astype(jnp.bfloat16)
    return (grad_input, grad_gain, grad_gate, grad_up, grad_down)


def solution(mesh):
    placed = (
        P("rep", ("fs", "tp")),
        P("rep", ("fs", "tp")),
        P(),
        P(("fs", "tp"), None),
        P(("fs", "tp"), None),
        P(("fs", "tp"), None),
    )
    return jax.shard_map(
        local,
        mesh=mesh,
        in_specs=placed,
        out_specs=(
            P("rep", ("fs", "tp")),
            P(("fs", "tp")),
            P(("fs", "tp"), None),
            P(("fs", "tp"), None),
            P(("fs", "tp"), None),
        ),
        check_vma=False,
    )
```

profile of v0, /device:TPU:0, one launch (start us, length us, event | category | flops | bytes accessed | tf_op | source)
XLA Modules:
  0.0 698.9 jit_solution(6119592157997108099)
XLA Ops:
  7.2 0.0 all-gather.3.cloned.1.call-start
  7.2 0.7 all-gather.3.cloned.1.call-update
  7.9 0.0 all-gather.5.cloned.1.call-start
  8.0 0.7 all-gather.5.cloned.1.call-update
  8.7 0.0 reduce-scatter.2.cloned.1.call-start
  8.7 29.7 %all-gather.3.cloned.1.call-done = bf16[384,2048]{1,0:T(8,128)(2,1)} async-done(((bf16[384,256]{1,0:T(8,128)(2,1)}), bf16[384,2048]{1,0:T(8,128)(2,1)}) %all-gather.3.cloned.1.call-update) | async-done | bytes 1572880 | tf_op jit(solution)/shard_map/all_gather | solution.py:23
  38.4 1.8 fusion
  40.2 5.1 fusion.12
  45.3 2.6 fusion.10
  48.0 18.1 %all-gather.5.cloned.1.call-done = bf16[384,2048]{1,0:T(8,128)(2,1)} async-done(((bf16[384,256]{1,0:T(8,128)(2,1)}), bf16[384,2048]{1,0:T(8,128)(2,1)}) %all-gather.5.cloned.1.call-update) | async-done | bytes 1572880 | tf_op jit(solution)/shard_map/all_gather | solution.py:24
  66.1 4.7 multiply_convert_fusion.1
  70.8 1.4 fusion.14
  72.3 0.5 copy-done.7
  72.8 3.2 convolution_add_fusion
  76.0 0.0 all-reduce.3.cloned.1.call-start
  76.1 1.3 copy-done.3
  77.4 0.1 copy-done.6
  77.5 4.2 fusion.6
  81.6 4.2 fusion.8
  85.8 4.1 convolution_multiply_fusion
  89.9 0.1 dynamic_slice.3
  90.0 32.2 %reduce-scatter.2.cloned.1.call-done = f32[384,256]{1,0:T(8,128)} async-done(((f32[384,2048]{1,0:T(8,128)}), f32[384,256]{1,0:T(8,128)}) %reduce-scatter.2.cloned.1.call-update) | async-done | bytes 393232 | tf_op jit(solution)/shard_map/reduce_scatter | solution.py:45
  122.2 1.2 multiply_reduce_fusion
  123.4 12.5 %psum.35 = f32[384]{0:T(512)S(1)} all-reduce(f32[384]{0:T(512)S(1)} %get-tuple-element.6), channel_id=1, replica_groups=mesh['rep'=4,'fs'=2,'tp'=4] {'fs','tp'}, use_global_device_ids=true, to_apply=%region_3.0 | all-reduce | flops 384 | bytes 3072 | tf_op jit(solution)/shard_map/psum | solution.py:52
  136.0 13.3 %psum.36 = f32[256]{0:T(256)} all-reduce(f32[256]{0:T(256)S(1)} %get-tuple-element.5), channel_id=1, replica_groups=mesh['rep'=4,'fs'=2,'tp'=4] {'rep'}, use_global_device_ids=true, to_apply=%region_5.0 | all-reduce | flops 256 | bytes 2048 | tf_op jit(solution)/shard_map/psum | solution.py:54
  149.3 1.9 add_convert_fusion
  151.1 528.1 %all-reduce.3.cloned.1.call-done = (f32[672,2048]{1,0:T(8,128)}, f32[672,2048]{1,0:T(8,128)}, f32[672,2048]{1,0:T(8,128)}) async-done(((f32[672,2048]{1,0:T(8,128)}, f32[672,2048]{1,0:T(8,128)}, f32[672,2048]{1,0:T(8,128)}), (f32[672,2048]{1,0:T(8,128)}, f32[672,2048]{1,0:T(8,128)}, f32[672,2048]{1,0:T(8,128)})) %all-reduce.3.cloned.1.call-update) | async-done | bytes 16515088 | tf_op jit(solution)/shard_map/psum | solution.py:54
  679.2 6.2 copy.14
  685.4 2.6 copy.15
  688.0 0.7 slice-done.1
  688.6 2.8 copy.16
  691.4 1.0 copy-done.1
  (32 shorter events, 0.1 us)
Async XLA Ops:
  7.2 38.1 %copy-start = (bf16[672,2048]{1,0:T(8,128)(2,1)S(1)}, bf16[672,2048]{1,0:T(8,128)(2,1)}, u32[]{:S(2)}) copy-start(bf16[672,2048]{1,0:T(8,128)(2,1)} %param.9) | copy-start | bytes 8257540
  7.2 31.2 %all-gather.3.cloned.1.call-start = ((), (), s32[]{:S(2)}) async-start(), calls=%async_computation.1 | async-start | bytes 1769472 | tf_op jit(solution)/shard_map/all_gather | solution.py:23
  7.9 58.2 %all-gather.5.cloned.1.call-start = ((), (), s32[]{:S(2)}) async-start(), calls=%async_computation.2 | async-start | bytes 1769472 | tf_op jit(solution)/shard_map/all_gather | solution.py:24
  8.7 113.5 %reduce-scatter.2.cloned.1.call-start = ((), (), s32[]{:S(2)}) async-start(), calls=%async_computation.3 | async-start | bytes 3538944 | tf_op jit(solution)/shard_map/reduce_scatter | solution.py:45
  40.2 5.1 copy-start.2
  40.2 5.1 copy-start.10
  70.8 1.5 copy-start.5
  70.8 2.0 copy-start.7
  76.0 1.4 copy-start.3
  76.0 1.5 copy-start.6
  76.0 603.2 %all-reduce.3.cloned.1.call-start = ((), (), s32[]{:S(2)}) async-start(), calls=%async_computation.4 | async-start | bytes 33030144 | tf_op jit(solution)/shard_map/psum | solution.py:54
  81.6 4.2 copy-start.11
  81.6 4.2 copy-start.12
  81.6 4.2 copy-start.13
  89.9 32.3 %copy-start.8 = (bf16[384,256]{1,0:T(8,128)(2,1)S(1)}, bf16[384,256]{1,0:T(8,128)(2,1)}, u32[]{:S(2)}) copy-start(bf16[384,256]{1,0:T(8,128)(2,1)} %param.6) | copy-start | bytes 589828
  89.9 59.4 %copy-start.9 = (bf16[384,256]{1,0:T(8,128)(2,1)S(1)}, bf16[384,256]{1,0:T(8,128)(2,1)}, u32[]{:S(2)}) copy-start(bf16[384,256]{1,0:T(8,128)(2,1)} %param.7) | copy-start | bytes 589828
  679.2 6.2 copy-start.4
  679.2 8.8 %slice-start = ((s8[5505024]{0:T(1024)(128)(4,1)}), s8[4194304]{0:T(1024)(128)(4,1)S(1)}, s32[]{:S(2)}) async-start(s8[5505024]{0:T(1024)(128)(4,1)} %bitcast.11), calls=%async_computation.5 | async-start | bytes 8388608
  685.4 3.2 slice-start.1
  688.6 3.8 copy-start.1
Sparse Core Ops, SparseCore 0:
  9.9 28.4 all-gather.2
  40.3 25.7 all-gather.4
  76.1 46.0 reduce-scatter.1
  125.5 553.7 all-reduce.2
where the time goes:
time: 699 us
  waiting for transfers between devices  610 us (87%)
  matrix products  29.4 us (4%)
  blocking collectives  25.8 us (4%)
  local copies, waits for them, and re-layouts  15.3 us (2%)
  between operations  13.9 us (2%)
    psum x1, waiting for transfers between devices, local(): lax.psum((grad_gate, grad_up, grad_down, gain_part), 'rep')  528 us
    reduce_scatter x1, waiting for transfers between devices, local(): lax.psum_scatter(partial_value, ('fs', 'tp'), scatter_dimension=1, tiled=...  32.2 us
    all_gather x1, waiting for transfers between devices, local(): lax.all_gather(tokens, ('fs', 'tp'), axis=1, tiled=True)  29.7 us
    all_gather x1, waiting for transfers between devices, local(): lax.all_gather(cotangent, ('fs', 'tp'), axis=1, tiled=True)  18.1 us
    unnamed x35, local copies, waits for them, and re-layouts  15.2 us
  transfers between devices with their start and end apart: 4, of which 4 were waited for; matrix products, arithmetic and copies ran while one was open for 4% of the time, Pallas kernels for 0%

commit v1 on v0

v1 whole, which is shorter than its diff:
```python
import jax
import jax.numpy as jnp
from jax import lax
from jax.sharding import PartitionSpec as P

EPS = 1e-06
PLANE = ("fs", "tp")


def right_product(left, weight):
    return lax.dot_general(
        left, weight, (((1,), (1,)), ((), ())), preferred_element_type=jnp.float32
    )


def left_product(left, right):
    return lax.dot_general(
        left, right, (((0,), (0,)), ((), ())), preferred_element_type=jnp.float32
    )


def normalise(x, gain):
    xf = x.astype(jnp.float32)
    inv_rms = lax.rsqrt(jnp.mean(xf * xf, axis=1, keepdims=True) + EPS)
    return inv_rms, (xf * inv_rms * gain).astype(jnp.bfloat16)


def hidden_grads(normed, dy, w_gate, w_up, w_down):
    gate = right_product(normed, w_gate)
    up = right_product(normed, w_up)
    sig = jax.nn.sigmoid(gate)
    active = gate * sig
    hidden = (active * up).astype(jnp.bfloat16)
    d_hidden = 0.5 * right_product(dy, w_down)
    d_gate = (d_hidden * up * sig * (1.0 + gate * (1.0 - sig))).astype(jnp.bfloat16)
    d_up = (d_hidden * active).astype(jnp.bfloat16)
    return hidden, d_gate, d_up


def input_grads(tokens, cotangent, gain, inv_rms, d_gate, d_up, w_gate, w_up, wire):
    partial_value = jnp.dot(d_gate, w_gate, preferred_element_type=jnp.float32) + jnp.dot(
        d_up, w_up, preferred_element_type=jnp.float32
    )
    width = partial_value.shape[1]
    summed = lax.psum_scatter(
        partial_value.astype(wire), PLANE, scatter_dimension=1, tiled=True
    ).astype(jnp.float32)
    own_width = summed.shape[1]
    unit_own = tokens.astype(jnp.float32) * inv_rms
    gain_own = lax.dynamic_slice_in_dim(
        gain, lax.axis_index(PLANE) * own_width, own_width, 0
    )
    d_unit = summed * gain_own
    row_mean = lax.psum(jnp.sum(unit_own * d_unit, axis=1), PLANE) / width
    gain_part = jnp.sum(unit_own * summed, axis=0)
    grad_input = (
        cotangent.astype(jnp.float32) + inv_rms * (d_unit - unit_own * row_mean[:, None])
    ).astype(jnp.bfloat16)
    return grad_input, gain_part


def reduced(tokens, cotangent, gain, w_gate, w_up, w_down):
    full_x = lax.all_gather(tokens, PLANE, axis=1, tiled=True)
    full_dy = lax.all_gather(cotangent, PLANE, axis=1, tiled=True)
    inv_rms, normed = normalise(full_x, gain)
    hidden, d_gate, d_up = hidden_grads(normed, full_dy, w_gate, w_up, w_down)
    grad_down = 0.5 * left_product(hidden, full_dy)
    grad_gate = left_product(d_gate, normed)
    grad_up = left_product(d_up, normed)
    grad_input, gain_part = input_grads(
        tokens, cotangent, gain, inv_rms, d_gate, d_up, w_gate, w_up, jnp.float32
    )
    grad_gate, grad_up, grad_down, grad_gain = lax.psum(
        (grad_gate, grad_up, grad_down, gain_part), "rep"
    )
    return (grad_input, grad_gain, grad_gate, grad_up, grad_down)


def gathered(tokens, cotangent, gain, w_gate, w_up, w_down):
    rows, cols = tokens.shape
    both = lax.all_gather(jnp.stack([tokens, cotangent]), ("rep",) + PLANE)
    reps = lax.axis_size("rep")
    plane = lax.axis_size(PLANE)
    both = both.reshape(reps, plane, 2, rows, cols).transpose(2, 0, 3, 1, 4)
    both = both.reshape(2, reps * rows, plane * cols)
    inv_rms, normed = normalise(both[0], gain)
    dy = both[1]
    hidden, d_gate, d_up = hidden_grads(normed, dy, w_gate, w_up, w_down)
    start = lax.axis_index("rep") * rows
    own = lambda a: lax.dynamic_slice_in_dim(a, start, rows, 0)
    grad_input, gain_part = input_grads(
        tokens, cotangent, gain, own(inv_rms), own(d_gate), own(d_up), w_gate, w_up, jnp.bfloat16
    )
    grad_down = 0.5 * left_product(hidden, dy)
    grad_gate = left_product(d_gate, normed)
    grad_up = left_product(d_up, normed)
    return (grad_input, lax.psum(gain_part, "rep"), grad_gate, grad_up, grad_down)


def local(tokens, cotangent, gain, w_gate, w_up, w_down):
    reps = lax.axis_size("rep")
    token_bytes = 2 * 2 * tokens.shape[0] * reps * w_gate.shape[1]
    grad_bytes = 3 * 4 * w_gate.size
    plan = gathered if token_bytes < grad_bytes else reduced
    return plan(tokens, cotangent, gain, w_gate, w_up, w_down)


def solution(mesh):
    placed = (
        P("rep", PLANE),
        P("rep", PLANE),
        P(),
        P(PLANE, None),
        P(PLANE, None),
        P(PLANE, None),
    )
    return jax.shard_map(
        local,
        mesh=mesh,
        in_specs=placed,
        out_specs=(
            P("rep", PLANE),
            P(PLANE),
            P(PLANE, None),
            P(PLANE, None),
            P(PLANE, None),
        ),
        check_vma=False,
    )
```

time: 699 us -> 270 us (0.39)
  waiting for transfers between devices: 610 us -> 118 us
  matrix products: 29.4 us -> 53.6 us
  local copies, waits for them, and re-layouts: 15.3 us -> 36.4 us
  other arithmetic: 4.89 us -> 23.8 us
    psum x1 -> x0, waiting for transfers between devices: 528 us -> none  [local(): lax.psum((grad_gate, grad_up, grad_down, gain_part), 'rep')]
    all_gather x2 -> x1, waiting for transfers between devices: 47.8 us -> 99.3 us  [gathered(): both = lax.all_gather(jnp.stack([tokens, cotangent]), ('rep',) + PLANE)]
    reduce_scatter x1, waiting for transfers between devices: 32.2 us -> 18.5 us  [input_grads(): lax.psum_scatter(partial_value.astype(wire), PLANE, scatter_dimension=1,...]
    dot_general x3, matrix products: 12.4 us -> 24.8 us  [right_product(): lax.dot_general(left, weight, (((1,), (1,)), ((), ())), preferred_element...]
    dot_general x3, matrix products: 12.4 us -> 24.7 us  [left_product(): lax.dot_general(left, right, (((0,), (0,)), ((), ())), preferred_element_...]
    reshape x0 -> x1, local copies, waits for them, and re-layouts: none -> 11.9 us  [gathered(): both = both.reshape(reps, plane, 2, rows, cols).transpose(2, 0, 3, 1, 4)]
    unnamed x35 -> x31, local copies, waits for them, and re-layouts: 15.2 us -> 23.6 us
    convert_element_type x1 -> x2, other arithmetic: 1.86 us -> 10.2 us  [the longest x1 8.35 us: normalise(): return (inv_rms, (xf * inv_rms * gain).astype(jnp.bfloat16))]
  transfers between devices with their start and end apart: 4 -> 2, of which waited for: 4 -> 2; matrix products, arithmetic and copies ran while one was open for 4% -> 7% of each run, Pallas kernels for 0% -> 0%
where the time goes in v1:
time: 270 us
  waiting for transfers between devices  118 us (44%)
  matrix products  53.6 us (20%)
  local copies, waits for them, and re-layouts  36.4 us (13%)
  blocking collectives  24 us (9%)
  other arithmetic  23.8 us (9%)
  between operations  14.2 us (5%)
    all_gather x1, waiting for transfers between devices, gathered(): both = lax.all_gather(jnp.stack([tokens, cotangent]), ('rep',) + PLANE)  99.3 us
    dot_general x3, matrix products, right_product(): lax.dot_general(left, weight, (((1,), (1,)), ((), ())), preferred_element...  24.8 us
    dot_general x3, matrix products, left_product(): lax.dot_general(left, right, (((0,), (0,)), ((), ())), preferred_element_...  24.7 us
    unnamed x31, local copies, waits for them, and re-layouts  23.6 us
    reduce_scatter x1, waiting for transfers between devices, input_grads(): lax.psum_scatter(partial_value.astype(wire), PLANE, scatter_dimension=1,...  18.5 us
    psum x1, blocking collectives, gathered(): lax.psum(gain_part, 'rep')  12.3 us
    reshape x1, local copies, waits for them, and re-layouts, gathered(): both = both.reshape(reps, plane, 2, rows, cols).transpose(2, 0, 3, 1, 4)  11.9 us
    psum x1, blocking collectives, input_grads(): row_mean = lax.psum(jnp.sum(unit_own * d_unit, axis=1), PLANE) / width  11.8 us
  transfers between devices with their start and end apart: 2, of which 2 were waited for; matrix products, arithmetic and copies ran while one was open for 7% of the time, Pallas kernels for 0%

profile of v1, /device:TPU:0, one launch (start us, length us, event | category | flops | bytes accessed | tf_op | source)
XLA Modules:
  0.0 269.9 jit_solution(12659345209265375576)
XLA Ops:
  7.2 0.0 copy-start
  7.2 0.0 all-gather.3.cloned.1.call-start
  7.2 2.0 pad_maximum_fusion
  9.2 0.0 all-gather.3.cloned.1.call-update
  9.2 0.0 reduce-scatter.2.cloned.1.call-start
  9.3 0.8 dynamic_slice.15
  10.0 99.3 %all-gather.3.cloned.1.call-done = bf16[64,384,256]{2,1,0:T(8,128)(2,1)} async-done(((bf16[2,384,256]{2,1,0:T(8,128)(2,1)}), bf16[64,384,256]{2,1,0:T(8,128)(2,1)}) %all-gather.3.cloned.1.call-update) | async-done | bytes 12582928 | tf_op jit(solution)/shard_map/all_gather | solution.py:81
  109.3 11.9 %copy.17 = bf16[4,8,2,384,256]{4,1,3,0,2:T(8,128)(2,1)S(1)} copy(bf16[4,8,2,384,256]{4,3,2,1,0:T(8,128)(2,1)} %bitcast.35) | data formatting | bytes 25165824 | tf_op jit(solution)/shard_map/reshape | solution.py:84
  121.3 3.5 %multiply_reduce_fusion = f32[4,384]{1,0:T(4,128)S(1)} fusion(bf16[2,4,384,8,256]{4,3,2,1,0:T(8,128)(2,1)S(1)} %bitcast.30), kind=kLoop, calls=%fused_computation.2 | loop fusion | flops 9435648 | bytes 6297600 | tf_op jit(solution)/shard_map/reduce_sum | solution.py:24
  124.8 6.9 %fusion.16 = (bf16[1,4,384,8,256]{4,3,2,1,0:T(8,128)(2,1)}, f32[1,4,384,8,256]{4,3,2,1,0:T(8,128)}) fusion(bf16[2,4,384,8,256]{4,3,2,1,0:T(8,128)(2,1)S(1)} %bitcast.31), kind=kLoop, calls=%fused_computation.32 | loop fusion | flops 3145728 | bytes 31457280 | tf_op jit(solution)/shard_map/slice | solution.py:87
  131.8 8.2 %copy.14 = bf16[192,8,8,256]{3,1,2,0:T(8,128)(2,1)} copy(bf16[192,8,8,256]{3,2,1,0:T(8,128)(2,1)} %bitcast.34) | data formatting | bytes 12582912
  140.0 15.3 %copy.15 = f32[192,8,8,256]{3,1,2,0:T(8,128)} copy(f32[192,8,8,256]{3,2,1,0:T(8,128)} %bitcast.32) | data formatting | bytes 25165824
  155.3 8.3 %multiply_convert_fusion = bf16[1536,2048]{1,0:T(8,128)(2,1)} fusion(f32[1536,2048]{1,0:T(8,128)} %bitcast.33, f32[2048]{0:T(1024)S(1)} %copy-done.9, f32[1536]{0:T(1024)S(1)} %rsqrt.20), kind=kLoop, calls=%fused_computation.1 | loop fusion | flops 9437184 | bytes 18888704 | tf_op jit(solution)/shard_map/convert_element_type | solution.py:25
  163.7 10.4 %fusion.18 = f32[1536,672]{0,1:T(8,128)} fusion(bf16[1536,2048]{1,0:T(8,128)(2,1)} %multiply_convert_fusion, bf16[672,2048]{1,0:T(8,128)(2,1)} %param.9), kind=kOutput, calls=%fused_computation.34 | convolution fusion | flops 4227858432 | bytes 13172736 | tf_op jit(solution)/shard_map/dot_general | solution.py:11
  174.1 6.2 %fusion.17 = f32[1536,672]{0,1:T(8,128)} fusion(bf16[1536,2048]{1,0:T(8,128)(2,1)S(1)} %copy-done.3, bf16[672,2048]{1,0:T(8,128)(2,1)S(1)} %copy-done.4), kind=kOutput, calls=%fused_computation.33 | convolution fusion | flops 4227858432 | bytes 13172736 | tf_op jit(solution)/shard_map/dot_general | solution.py:11
  180.3 0.0 copy-start.2
  180.4 8.2 %multiply_convert_fusion.2 = (bf16[1536,672]{0,1:T(8,128)(2,1)S(1)}, bf16[1536,672]{0,1:T(8,128)(2,1)S(1)}) fusion(f32[1536,672]{0,1:T(8,128)} %fusion.18, f32[1536,672]{0,1:T(8,128)} %fusion.17, bf16[1536,2048]{1,0:T(8,128)(2,1)S(1)} %bitcast.39, bf16[672,2048]{1,0:T(8,128)(2,1)S(1)} %copy-done), kind=kOutput, calls=%fused_computation.5 | convolution fusion | flops 4242309120 | bytes 21430272 | tf_op jit(solution)/shard_map/dot_general | solution.py:11
  188.6 0.0 copy-start.7
  188.6 1.4 fusion.3
  190.1 6.2 %fusion.20 = f32[672,2048]{1,0:T(8,128)} fusion(bf16[1536,672]{0,1:T(8,128)(2,1)S(1)} %get-tuple-element.9, bf16[1536,2048]{1,0:T(8,128)(2,1)S(1)} %copy-done.3), kind=kOutput, calls=%fused_computation.36 | convolution fusion | flops 4227858432 | bytes 13860864 | tf_op jit(solution)/shard_map/dot_general | solution.py:17
  196.2 2.6 add_convert_fusion
  198.8 0.0 reduce-scatter.2.cloned.1.call-update
  198.9 0.0 copy-start.10
  198.9 9.1 %fusion.19 = f32[672,2048]{1,0:T(8,128)} fusion(bf16[1536,672]{0,1:T(8,128)(2,1)S(1)} %copy-done.8, bf16[1536,2048]{1,0:T(8,128)(2,1)} %multiply_convert_fusion), kind=kOutput, calls=%fused_computation.35 | convolution fusion | flops 4227858432 | bytes 13860864 | tf_op jit(solution)/shard_map/dot_general | solution.py:17
  208.0 0.0 copy-start.6
  208.0 0.0 copy-start.1
  208.0 9.5 %convolution_multiply_fusion = f32[672,2048]{1,0:T(8,128)} fusion(bf16[1536,2048]{1,0:T(8,128)(2,1)} %bitcast.36, f32[1536,672]{0,1:T(8,128)S(1)} %copy-done.11, f32[1536,672]{0,1:T(8,128)S(1)} %copy-done.10), kind=kOutput, calls=%fused_computation.9 | convolution fusion | flops 4235427840 | bytes 20054016 | tf_op jit(solution)/shard_map/dot_general | solution.py:17
  217.5 18.5 %reduce-scatter.2.cloned.1.call-done = bf16[384,256]{1,0:T(8,128)(2,1)} async-done(((bf16[384,2048]{1,0:T(8,128)(2,1)}), bf16[384,256]{1,0:T(8,128)(2,1)}) %reduce-scatter.2.cloned.1.call-update) | async-done | bytes 196624 | tf_op jit(solution)/shard_map/reduce_scatter | solution.py:45
  236.0 1.2 fusion.11
  237.2 12.3 %psum.15 = f32[256]{0:T(256)} all-reduce(f32[256]{0:T(256)S(1)} %get-tuple-element.5), channel_id=1, replica_groups=mesh['rep'=4,'fs'=2,'tp'=4] {'rep'}, use_global_device_ids=true, to_apply=%region_5.0 | all-reduce | flops 256 | bytes 2048 | tf_op jit(solution)/shard_map/psum | solution.py:97
  249.4 11.8 %psum.14 = f32[384]{0:T(512)S(1)} all-reduce(f32[384]{0:T(512)S(1)} %get-tuple-element.6), channel_id=1, replica_groups=mesh['rep'=4,'fs'=2,'tp'=4] {'fs','tp'}, use_global_device_ids=true, to_apply=%region_3.0 | all-reduce | flops 384 | bytes 3072 | tf_op jit(solution)/shard_map/psum | solution.py:54
  261.2 1.8 fusion.10
  (28 shorter events, 0.1 us)
Async XLA Ops:
  7.2 173.2 %copy-start = (bf16[672,2048]{1,0:T(8,128)(2,1)S(1)}, bf16[672,2048]{1,0:T(8,128)(2,1)}, u32[]{:S(2)}) copy-start(bf16[672,2048]{1,0:T(8,128)(2,1)} %param.11) | copy-start | bytes 8257540
  7.2 102.2 %all-gather.3.cloned.1.call-start = ((), (), s32[]{:S(2)}) async-start(), calls=%async_computation.2 | async-start | bytes 12976128 | tf_op jit(solution)/shard_map/all_gather | solution.py:81
  9.2 226.8 %reduce-scatter.2.cloned.1.call-start = ((), (), s32[]{:S(2)}) async-start(), calls=%async_computation.1 | async-start | bytes 1769472 | tf_op jit(solution)/shard_map/reduce_scatter | solution.py:45
  140.0 15.3 %copy-start.9 = (f32[2048]{0:T(1024)S(1)}, f32[2048]{0:T(1024)}, u32[]{:S(2)}) copy-start(f32[2048]{0:T(1024)} %param.8) | copy-start | bytes 24580
  163.7 10.4 %copy-start.3 = (bf16[1536,2048]{1,0:T(8,128)(2,1)S(1)}, bf16[1536,2048]{1,0:T(8,128)(2,1)}, u32[]{:S(2)}) copy-start(bf16[1536,2048]{1,0:T(8,128)(2,1)} %multiply_convert_fusion) | copy-start | bytes 18874372
  163.7 10.4 %copy-start.4 = (bf16[672,2048]{1,0:T(8,128)(2,1)S(1)}, bf16[672,2048]{1,0:T(8,128)(2,1)}, u32[]{:S(2)}) copy-start(bf16[672,2048]{1,0:T(8,128)(2,1)} %param.10) | copy-start | bytes 8257540
  163.7 16.6 %slice-start = ((s8[6291456]{0:T(1024)(128)(4,1)}), s8[4194304]{0:T(1024)(128)(4,1)S(1)}, s32[]{:S(2)}) async-start(s8[6291456]{0:T(1024)(128)(4,1)} %bitcast.37), calls=%async_computation.3 | async-start | bytes 8388608
  174.1 6.2 %slice-start.1 = ((s8[6291456]{0:T(1024)(128)(4,1)}), s8[2097152]{0:T(1024)(128)(4,1)S(1)}, s32[]{:S(2)}) async-start(s8[6291456]{0:T(1024)(128)(4,1)} %bitcast.37), calls=%async_computation.4 | async-start | bytes 4194304
  180.3 8.3 %copy-start.2 = (bf16[672,2048]{1,0:T(8,128)(2,1)S(1)}, bf16[672,2048]{1,0:T(8,128)(2,1)}, u32[]{:S(2)}) copy-start(bf16[672,2048]{1,0:T(8,128)(2,1)} %param.9) | copy-start | bytes 8257540
  188.6 1.5 copy-start.7
  196.2 2.6 copy-start.8
  198.9 9.1 %copy-start.10 = (f32[1536,672]{0,1:T(8,128)S(1)}, f32[1536,672]{0,1:T(8,128)}, u32[]{:S(2)}) copy-start(f32[1536,672]{0,1:T(8,128)} %fusion.18) | copy-start | bytes 12386308
  198.9 9.1 %copy-start.11 = (f32[1536,672]{0,1:T(8,128)S(1)}, f32[1536,672]{0,1:T(8,128)}, u32[]{:S(2)}) copy-start(f32[1536,672]{0,1:T(8,128)} %fusion.17) | copy-start | bytes 12386308
  208.0 28.0 %copy-start.5 = (bf16[384,256]{1,0:T(8,128)(2,1)S(1)}, bf16[384,256]{1,0:T(8,128)(2,1)}, u32[]{:S(2)}) copy-start(bf16[384,256]{1,0:T(8,128)(2,1)} %param.6) | copy-start | bytes 589828
  208.0 53.2 %copy-start.6 = (bf16[384,256]{1,0:T(8,128)(2,1)S(1)}, bf16[384,256]{1,0:T(8,128)(2,1)}, u32[]{:S(2)}) copy-start(bf16[384,256]{1,0:T(8,128)(2,1)} %param.7) | copy-start | bytes 589828
  208.0 55.0 %copy-start.1 = (bf16[672,2048]{1,0:T(8,128)(2,1)S(1)}, bf16[672,2048]{1,0:T(8,128)(2,1)}, u32[]{:S(2)}) copy-start(bf16[672,2048]{1,0:T(8,128)(2,1)} %param.11) | copy-start | bytes 8257540
Sparse Core Ops, SparseCore 0:
  11.4 97.8 all-gather.2
  199.0 36.9 reduce-scatter.1

commit v2 on v1

--- a/solution.py
+++ b/solution.py
@@ -1,6 +1,10 @@
+import functools
+
 import jax
 import jax.numpy as jnp
 from jax import lax
+from jax.experimental import pallas as pl
+from jax.experimental.pallas import tpu as pltpu
 from jax.sharding import PartitionSpec as P
 
 EPS = 1e-06
@@ -37,13 +41,30 @@
     return hidden, d_gate, d_up
 
 
-def input_grads(tokens, cotangent, gain, inv_rms, d_gate, d_up, w_gate, w_up, wire):
-    partial_value = jnp.dot(d_gate, w_gate, preferred_element_type=jnp.float32) + jnp.dot(
+def hidden_sum(d_gate, d_up, w_gate, w_up):
+    return jnp.dot(d_gate, w_gate, preferred_element_type=jnp.float32) + jnp.dot(
         d_up, w_up, preferred_element_type=jnp.float32
     )
+
+
+def slotted_sums(rows_part, gain_part):
+    rep, spot = lax.axis_index("rep"), lax.axis_index(PLANE)
+    reps, plane = lax.axis_size("rep"), lax.axis_size(PLANE)
+    rows, cols = rows_part.shape[0], gain_part.shape[0]
+    slots = jnp.zeros((reps * rows + plane * cols,), jnp.float32)
+    slots = lax.dynamic_update_slice(slots, rows_part, (rep * rows,))
+    slots = lax.dynamic_update_slice(slots, gain_part, (reps * rows + spot * cols,))
+    slots = lax.psum(slots, ("rep",) + PLANE)
+    return (
+        lax.dynamic_slice(slots, (rep * rows,), (rows,)),
+        lax.dynamic_slice(slots, (reps * rows + spot * cols,), (cols,)),
+    )
+
+
+def input_grads(tokens, cotangent, gain, inv_rms, partial_value, sums):
     width = partial_value.shape[1]
     summed = lax.psum_scatter(
-        partial_value.astype(wire), PLANE, scatter_dimension=1, tiled=True
+        partial_value, PLANE, scatter_dimension=1, tiled=True
     ).astype(jnp.float32)
     own_width = summed.shape[1]
     unit_own = tokens.astype(jnp.float32) * inv_rms
@@ -51,8 +72,8 @@
         gain, lax.axis_index(PLANE) * own_width, own_width, 0
     )
     d_unit = summed * gain_own
-    row_mean = lax.psum(jnp.sum(unit_own * d_unit, axis=1), PLANE) / width
-    gain_part = jnp.sum(unit_own * summed, axis=0)
+    row_sum, gain_part = sums(jnp.sum(unit_own * d_unit, axis=1), jnp.sum(unit_own * summed, axis=0))
+    row_mean = row_sum / width
     grad_input = (
         cotangent.astype(jnp.float32) + inv_rms * (d_unit - unit_own * row_mean[:, None])
     ).astype(jnp.bfloat16)
@@ -68,7 +89,8 @@
     grad_gate = left_product(d_gate, normed)
     grad_up = left_product(d_up, normed)
     grad_input, gain_part = input_grads(
-        tokens, cotangent, gain, inv_rms, d_gate, d_up, w_gate, w_up, jnp.float32
+        tokens, cotangent, gain, inv_rms, hidden_sum(d_gate, d_up, w_gate, w_up),
+        lambda rows_part, gain_part: (lax.psum(rows_part, PLANE), gain_part),
     )
     grad_gate, grad_up, grad_down, grad_gain = lax.psum(
         (grad_gate, grad_up, grad_down, gain_part), "rep"
@@ -76,25 +98,204 @@
     return (grad_input, grad_gain, grad_gate, grad_up, grad_down)
 
 
+def gather_kernel(reps, tps, x_ref, dy_ref, out_ref, buf, send_sem, recv_sem, pair_sem, in_sem, out_sem):
+    z, y, t = lax.axis_index("rep"), lax.axis_index("fs"), lax.axis_index("tp")
+    rows, cols = x_ref.shape
+    x_id = (z, y, lax.rem(t + 2, tps))
+    y_id = (z, 1 - y, t)
+    pair_id = (z, y, t + 1 - 2 * lax.rem(t, 2))
+    up_id, down_id = (z + 1, y, t), (z - 1, y, t)
+    has_up, has_down = z < reps - 1, z > 0
+    column = (
+        y * tps + t,
+        y * tps + lax.rem(t + 2, tps),
+        (1 - y) * tps + t,
+        (1 - y) * tps + lax.rem(t + 2, tps),
+    )
+    pair_column = tuple(c + 1 - 2 * lax.rem(t, 2) for c in column)
+
+    def piece(level, col, p):
+        return buf.at[
+            p,
+            pl.ds(pl.multiple_of(level * rows, rows), rows),
+            pl.ds(pl.multiple_of(col * cols, cols), cols),
+        ]
+
+    def copy(level, q, p, kind, target, landing):
+        ref = piece(level, column[q], p)
+        return pltpu.make_async_remote_copy(
+            src_ref=ref, dst_ref=ref, send_sem=send_sem.at[kind, level, p], recv_sem=landing,
+            device_id=target, device_id_type=pl.DeviceIdType.MESH,
+        )
+
+    def to_x(level, p):
+        return copy(level, 0, p, 0, x_id, recv_sem.at[1, level, p])
+
+    def to_y(level, p):
+        return copy(level, 0, p, 1, y_id, recv_sem.at[2, level, p])
+
+    def to_pair(level, q, p):
+        return copy(level, q, p, 2 + q, pair_id, pair_sem.at[q, level, p])
+
+    def to_up(level, p):
+        return copy(level, 0, p, 6, up_id, recv_sem.at[0, level, p])
+
+    def to_down(level, p):
+        return copy(level, 0, p, 7, down_id, recv_sem.at[0, level, p])
+
+    def corner(level, p):
+        if p == 0:
+            return copy(level, 1, p, 8, y_id, recv_sem.at[3, level, p])
+        return copy(level, 2, p, 8, x_id, recv_sem.at[3, level, p])
+
+    def landed(level, q, p):
+        copy(level, q, p, 0, x_id, recv_sem.at[q, level, p]).wait_recv()
+
+    loads = [
+        pltpu.make_async_copy(ref, piece(z, column[0], p), in_sem.at[p])
+        for p, ref in enumerate((x_ref, dy_ref))
+    ]
+    for load in loads:
+        load.start()
+    barrier = pltpu.get_barrier_semaphore()
+
+    def greet(target):
+        pl.semaphore_signal(barrier, inc=1, device_id=target, device_id_type=pl.DeviceIdType.MESH)
+
+    for target in (x_id, y_id, pair_id):
+        greet(target)
+    pl.when(has_up)(lambda: greet(up_id))
+    pl.when(has_down)(lambda: greet(down_id))
+    along_z = lax.div(z + reps - 1, reps) + lax.div(2 * reps - 2 - z, reps)
+    pl.semaphore_wait(barrier, 3 + along_z)
+
+    for p in range(2):
+        loads[p].wait()
+        pl.when(has_up)(lambda p=p: to_up(z, p).start())
+        pl.when(has_down)(lambda p=p: to_down(z, p).start())
+        to_x(z, p).start()
+        to_y(z, p).start()
+        to_pair(z, 0, p).start()
+
+    for far in range(1, reps):
+        for p in range(2):
+
+            @pl.when(z + far < reps)
+            def _():
+                level = z + far
+                landed(level, 0, p)
+                pl.when(has_down)(lambda: to_down(level, p).start())
+                to_x(level, p).start()
+                to_y(level, p).start()
+                to_pair(level, 0, p).start()
+
+            @pl.when(z - far >= 0)
+            def _():
+                level = z - far
+                landed(level, 0, p)
+                pl.when(has_up)(lambda: to_up(level, p).start())
+                to_x(level, p).start()
+                to_y(level, p).start()
+                to_pair(level, 0, p).start()
+
+    def each_level(act):
+        act(z)
+        for far in range(1, reps):
+            pl.when(z + far < reps)(lambda far=far: act(z + far))
+            pl.when(z - far >= 0)(lambda far=far: act(z - far))
+
+    def relay(level):
+        for q, p in ((1, 0), (2, 0), (1, 1), (2, 1)):
+            landed(level, q, p)
+            if q == p + 1:
+                corner(level, p).start()
+            to_pair(level, q, p).start()
+
+    def corners(level):
+        for p in range(2):
+            landed(level, 3, p)
+            to_pair(level, 3, p).start()
+
+    def store(level, p):
+        window = pl.ds(pl.multiple_of(level * rows, rows), rows)
+        return pltpu.make_async_copy(
+            buf.at[p, window], out_ref.at[p, window], out_sem.at[level, p]
+        )
+
+    def finish(level):
+        for p in range(2):
+            for q in range(4):
+                ref = piece(level, pair_column[q], p)
+                pltpu.make_async_remote_copy(
+                    src_ref=ref, dst_ref=ref, send_sem=send_sem.at[2 + q, level, p],
+                    recv_sem=pair_sem.at[q, level, p],
+                    device_id=pair_id, device_id_type=pl.DeviceIdType.MESH,
+                ).wait_recv()
+            store(level, p).start()
+
+    def drain(level):
+        for p in range(2):
+            to_x(level, p).wait_send()
+            to_y(level, p).wait_send()
+            corner(level, p).wait_send()
+            for q in range(4):
+                to_pair(level, q, p).wait_send()
+            pl.when(jnp.logical_and(has_up, level <= z))(lambda p=p: to_up(level, p).wait_send())
+            pl.when(jnp.logical_and(has_down, level >= z))(lambda p=p: to_down(level, p).wait_send())
+            store(level, p).wait()
+
+    for act in (relay, corners, finish, drain):
+        each_level(act)
+
+
+def gather_all(tokens, cotangent):
+    reps, fss, tps = (lax.axis_size(name) for name in ("rep", "fs", "tp"))
+    rows, cols = tokens.shape
+    shape = (2, reps * rows, fss * tps * cols)
+    return pl.pallas_call(
+        functools.partial(gather_kernel, reps, tps),
+        out_shape=jax.ShapeDtypeStruct(shape, tokens.dtype),
+        in_specs=[pl.BlockSpec(memory_space=pl.ANY)] * 2,
+        out_specs=pl.BlockSpec(memory_space=pl.ANY),
+        scratch_shapes=[
+            pltpu.VMEM(shape, tokens.dtype),
+            pltpu.SemaphoreType.DMA((9, reps, 2)),
+            pltpu.SemaphoreType.DMA((4, reps, 2)),
+            pltpu.SemaphoreType.DMA((4, reps, 2)),
+            pltpu.SemaphoreType.DMA((2,)),
+            pltpu.SemaphoreType.DMA((reps, 2)),
+        ],
+        compiler_params=pltpu.CompilerParams(
+            collective_id=0, has_side_effects=True, vmem_limit_bytes=48 * 2**20
+        ),
+    )(tokens, cotangent)
+
+
 def gathered(tokens, cotangent, gain, w_gate, w_up, w_down):
     rows, cols = tokens.shape
-    both = lax.all_gather(jnp.stack([tokens, cotangent]), ("rep",) + PLANE)
-    reps = lax.axis_size("rep")
-    plane = lax.axis_size(PLANE)
-    both = both.reshape(reps, plane, 2, rows, cols).transpose(2, 0, 3, 1, 4)
-    both = both.reshape(2, reps * rows, plane * cols)
+    if (lax.axis_size("fs"), lax.axis_size("tp")) == (2, 4) and cols % 128 == 0:
+        both = gather_all(tokens, cotangent)
+    else:
+        reps, plane = lax.axis_size("rep"), lax.axis_size(PLANE)
+        both = lax.all_gather(jnp.stack([tokens, cotangent]), ("rep",) + PLANE)
+        both = both.reshape(reps, plane, 2, rows, cols).transpose(2, 0, 3, 1, 4)
+        both = both.reshape(2, reps * rows, plane * cols)
     inv_rms, normed = normalise(both[0], gain)
     dy = both[1]
     hidden, d_gate, d_up = hidden_grads(normed, dy, w_gate, w_up, w_down)
     start = lax.axis_index("rep") * rows
     own = lambda a: lax.dynamic_slice_in_dim(a, start, rows, 0)
-    grad_input, gain_part = input_grads(
-        tokens, cotangent, gain, own(inv_rms), own(d_gate), own(d_up), w_gate, w_up, jnp.bfloat16
+    partial_value = hidden_sum(own(d_gate), own(d_up), w_gate, w_up).astype(jnp.bfloat16)
+    partial_value, hidden, d_gate, d_up = lax.optimization_barrier(
+        (partial_value, hidden, d_gate, d_up)
+    )
+    grad_input, grad_gain = input_grads(
+        tokens, cotangent, gain, own(inv_rms), partial_value, slotted_sums
     )
     grad_down = 0.5 * left_product(hidden, dy)
     grad_gate = left_product(d_gate, normed)
     grad_up = left_product(d_up, normed)
-    return (grad_input, lax.psum(gain_part, "rep"), grad_gate, grad_up, grad_down)
+    return (grad_input, grad_gain, grad_gate, grad_up, grad_down)
 
 
 def local(tokens, cotangent, gain, w_gate, w_up, w_down):

time: 270 us -> 195 us (0.72)
  waiting for transfers between devices: 118 us -> 7.37 us
  Pallas kernels: 0 us -> 61.6 us
  local copies, waits for them, and re-layouts: 36.4 us -> 3.85 us
  other arithmetic: 23.8 us -> 7.29 us
  blocking collectives: 24 us -> 39.4 us
  matrix products: 53.6 us -> 61.1 us
    all_gather x1 -> x0, waiting for transfers between devices: 99.3 us -> none  [gathered(): both = lax.all_gather(jnp.stack([tokens, cotangent]), ('rep',) + PLANE)]
    pallas_call x0 -> x1, Pallas kernels: none -> 61.6 us  [gather_all(): pl.pallas_call(functools.partial(gather_kernel, reps, tps), out_shape=jax...]
    unnamed x31 -> x24, local copies, waits for them, and re-layouts: 23.6 us -> 2.53 us
    psum x2 -> x1, blocking collectives: 24 us -> 39.4 us  [slotted_sums(): slots = lax.psum(slots, ('rep',) + PLANE)]
    reshape x1 -> x0, local copies, waits for them, and re-layouts: 11.9 us -> none  [gathered(): both = both.reshape(reps, plane, 2, rows, cols).transpose(2, 0, 3, 1, 4)]
    reduce_scatter x1, waiting for transfers between devices: 18.5 us -> 7.36 us  [input_grads(): lax.psum_scatter(partial_value, PLANE, scatter_dimension=1, tiled=True)]
    convert_element_type x1 -> x0, other arithmetic: 8.35 us -> none  [normalise(): return (inv_rms, (xf * inv_rms * gain).astype(jnp.bfloat16))]
    slice x1 -> x0, other arithmetic: 6.94 us -> none  [gathered(): dy = both[1]]
  transfers between devices with their start and end apart: 2 -> 1, of which waited for: 2 -> 1; matrix products, arithmetic and copies ran while one was open for 7% -> 16% of each run, Pallas kernels for 0% -> 0%
where the time goes in v2:
time: 195 us
  Pallas kernels  61.6 us (32%)
  matrix products  61.1 us (31%)
  blocking collectives  39.4 us (20%)
  between operations  14.2 us (7%)
  waiting for transfers between devices  7.37 us (4%)
  other arithmetic  7.29 us (4%)
  local copies, waits for them, and re-layouts  3.85 us (2%)
    pallas_call x1, Pallas kernels, gather_all(): pl.pallas_call(functools.partial(gather_kernel, reps, tps), out_shape=jax...  61.6 us
    psum x1, blocking collectives, slotted_sums(): slots = lax.psum(slots, ('rep',) + PLANE)  39.4 us
    dot_general x3, matrix products, left_product(): lax.dot_general(left, right, (((0,), (0,)), ((), ())), preferred_element_...  31 us
    dot_general x3, matrix products, right_product(): lax.dot_general(left, weight, (((1,), (1,)), ((), ())), preferred_element...  26 us
    reduce_scatter x1, waiting for transfers between devices, input_grads(): lax.psum_scatter(partial_value, PLANE, scatter_dimension=1, tiled=True)  7.36 us
    reduce_sum x1, other arithmetic, normalise(): inv_rms = lax.rsqrt(jnp.mean(xf * xf, axis=1, keepdims=True) + EPS)  4.23 us
  transfers between devices with their start and end apart: 1, of which 1 were waited for; matrix products, arithmetic and copies ran while one was open for 16% of the time, Pallas kernels for 0%

profile of v2, /device:TPU:0, one launch (start us, length us, event | category | flops | bytes accessed | tf_op | source)
XLA Modules:
  0.0 194.8 jit_solution(13762569409947979769)
XLA Ops:
  7.2 0.0 copy-start
  7.2 0.0 reduce-scatter.2.cloned.1.call-start
  7.2 0.0 copy-start.1
  7.2 1.1 copy-done.1
  8.3 0.9 copy-done.3
  9.2 61.6 %shard_map.101 = bf16[2,1536,2048]{2,1,0:T(8,128)(2,1)} custom-call(bf16[384,256]{1,0:T(8,128)(2,1)S(1)} %copy-done.1, bf16[384,256]{1,0:T(8,128)(2,1)S(1)} %copy-done.3), custom_call_target="tpu_custom_call" | custom-call | tf_op jit(solution)/shard_map/pallas_call | solution.py:255
  70.8 0.0 copy-start.10
  70.8 4.2 %fusion = f32[1536]{0:T(1024)S(1)} fusion(bf16[2,1536,2048]{2,1,0:T(8,128)(2,1)} %shard_map.101), kind=kLoop, calls=%fused_computation.2 | loop fusion | flops 9435648 | bytes 6297600 | tf_op jit(solution)/shard_map/reduce_sum | solution.py:28
  75.1 0.0 copy-done.10
  75.1 0.0 copy-start.9
  75.1 8.8 %fusion.5 = f32[1536,672]{0,1:T(8,128)} fusion(bf16[672,2048]{1,0:T(8,128)(2,1)S(1)} %copy-done.10, bf16[2,1536,2048]{2,1,0:T(8,128)(2,1)} %shard_map.101), kind=kOutput, calls=%fused_computation.7 | convolution fusion | flops 4227858432 | bytes 13172736 | tf_op jit(solution)/shard_map/dot_general | solution.py:15
  83.9 7.8 %fusion.29 = f32[1536,672]{0,1:T(8,128)S(1)} fusion(bf16[672,2048]{1,0:T(8,128)(2,1)} %param.9, f32[2048]{0:T(1024)S(1)} %copy-done.9, f32[1536]{0:T(1024)S(1)} %add_rsqrt_fusion, bf16[2,1536,2048]{2,1,0:T(8,128)(2,1)} %shard_map.101), kind=kOutput, calls=%fused_computation.37 | convolution fusion | flops 4240441344 | bytes 13187072 | tf_op jit(solution)/shard_map/dot_general | solution.py:15
  91.7 0.0 copy-done
  91.7 0.0 copy-start.5
  91.7 9.4 %multiply_convert_fusion = (bf16[1536,672]{0,1:T(8,128)(2,1)}, bf16[1536,672]{0,1:T(8,128)(2,1)S(1)}, bf16[1536,672]{0,1:T(8,128)(2,1)S(1)}) fusion(f32[1536,672]{0,1:T(8,128)S(1)} %fusion.29, f32[1536,672]{0,1:T(8,128)S(1)} %copy-done.11, bf16[672,2048]{1,0:T(8,128)(2,1)S(1)} %copy-done, f32[2048]{0:T(1024)S(1)} %copy-done.9, f32[1536]{0:T(1024)S(1)} %add_rsqrt_fusion, ...), kind=kOutput, calls=%fused_computation.11 | convolution fusion | flops 4256956416 | bytes 23508992 | tf_op jit(solution)/shard_map/dot_general | solution.py:15
  101.2 1.4 fusion.14
  102.6 0.5 copy-done.6
  103.1 2.7 %add_convert_fusion = bf16[384,2048]{1,0:T(8,128)(2,1)} fusion(f32[384,2048]{1,0:T(8,128)S(1)} %fusion.14, bf16[672,2048]{1,0:T(8,128)(2,1)S(1)} %copy-done, bf16[1536,672]{0,1:T(8,128)(2,1)S(1)} %get-tuple-element.11, s32[]{:T(128)S(6)} %select_n.16), kind=kOutput, calls=%fused_computation.17 | convolution fusion | flops 1058537472 | bytes 7987204 | tf_op jit(solution)/shard_map/dot_general | solution.py:45
  105.8 0.0 reduce-scatter.2.cloned.1.call-update
  105.8 10.3 %fusion.10 = f32[672,2048]{1,0:T(8,128)} fusion(bf16[1536,672]{0,1:T(8,128)(2,1)} %get-tuple-element.12, bf16[2,1536,2048]{2,1,0:T(8,128)(2,1)} %shard_map.101), kind=kOutput, calls=%fused_computation.16 | convolution fusion | flops 4229234688 | bytes 13860864 | tf_op jit(solution)/shard_map/dot_general | solution.py:21
  116.1 0.1 dynamic-slice.3
  116.1 0.1 dynamic_slice.18
  116.2 10.7 %fusion.27 = f32[672,2048]{1,0:T(8,128)} fusion(bf16[1536,672]{0,1:T(8,128)(2,1)} %copy-done.8, f32[2048]{0:T(1024)S(1)} %copy-done.9, f32[1536]{0:T(1024)S(1)} %add_rsqrt_fusion, bf16[2,1536,2048]{2,1,0:T(8,128)(2,1)} %shard_map.101), kind=kOutput, calls=%fused_computation.36 | convolution fusion | flops 4240441344 | bytes 13875200 | tf_op jit(solution)/shard_map/dot_general | solution.py:21
  127.0 10.0 %fusion.25 = f32[672,2048]{1,0:T(8,128)} fusion(bf16[1536,672]{0,1:T(8,128)(2,1)S(1)} %copy-done.7, f32[2048]{0:T(1024)S(1)} %copy-done.9, f32[1536]{0:T(1024)S(1)} %add_rsqrt_fusion, bf16[2,1536,2048]{2,1,0:T(8,128)(2,1)} %shard_map.101), kind=kOutput, calls=%fused_computation.35 | convolution fusion | flops 4240441344 | bytes 13875200 | tf_op jit(solution)/shard_map/dot_general | solution.py:21
  136.9 7.4 %reduce-scatter.2.cloned.1.call-done = bf16[384,256]{1,0:T(8,128)(2,1)} async-done(((bf16[384,2048]{1,0:T(8,128)(2,1)}), bf16[384,256]{1,0:T(8,128)(2,1)}) %reduce-scatter.2.cloned.1.call-update) | async-done | bytes 196624 | tf_op jit(solution)/shard_map/reduce_scatter | solution.py:66
  144.3 1.2 fusion.22
  145.5 0.3 dynamic_update_slice.6
  145.8 0.3 dynamic_update_slice.7
  146.0 39.4 %psum.7 = f32[3584]{0:T(1024)S(1)} all-reduce(f32[3584]{0:T(1024)S(1)} %dynamic_update_slice.7), channel_id=1, replica_groups=mesh['rep'=4,'fs'=2,'tp'=4] {'rep','fs','tp'}, use_global_device_ids=true, to_apply=%region_4.0 | all-reduce | flops 3584 | bytes 28672 | tf_op jit(solution)/shard_map/psum | solution.py:57
  185.4 0.6 dynamic_slice.20
  186.0 0.1 dynamic-slice_multiply_fusion
  186.1 1.8 fusion.21
  (16 shorter events, 0.0 us)
Async XLA Ops:
  7.2 84.5 %copy-start = (bf16[672,2048]{1,0:T(8,128)(2,1)S(1)}, bf16[672,2048]{1,0:T(8,128)(2,1)}, u32[]{:S(2)}) copy-start(bf16[672,2048]{1,0:T(8,128)(2,1)} %param.10) | copy-start | bytes 8257540
  7.2 137.1 %reduce-scatter.2.cloned.1.call-start = ((), (), s32[]{:S(2)}) async-start(), calls=%async_computation.1 | async-start | bytes 1769472 | tf_op jit(solution)/shard_map/reduce_scatter | solution.py:66
  7.2 1.1 copy-start.1
  8.3 0.9 copy-start.3
  70.8 4.3 %copy-start.10 = (bf16[672,2048]{1,0:T(8,128)(2,1)S(1)}, bf16[672,2048]{1,0:T(8,128)(2,1)}, u32[]{:S(2)}) copy-start(bf16[672,2048]{1,0:T(8,128)(2,1)} %param.11) | copy-start | bytes 8257540
  75.1 8.8 %copy-start.9 = (f32[2048]{0:T(1024)S(1)}, f32[2048]{0:T(1024)}, u32[]{:S(2)}) copy-start(f32[2048]{0:T(1024)} %param.8) | copy-start | bytes 24580
  83.9 7.8 %copy-start.11 = (f32[1536,672]{0,1:T(8,128)S(1)}, f32[1536,672]{0,1:T(8,128)}, u32[]{:S(2)}) copy-start(f32[1536,672]{0,1:T(8,128)} %fusion.5) | copy-start | bytes 12386308
  91.7 9.5 %copy-start.5 = (bf16[672,2048]{1,0:T(8,128)(2,1)S(1)}, bf16[672,2048]{1,0:T(8,128)(2,1)}, u32[]{:S(2)}) copy-start(bf16[672,2048]{1,0:T(8,128)(2,1)} %param.9) | copy-start | bytes 8257540
  101.2 1.4 copy-start.8
  101.2 1.9 copy-start.6
  116.2 10.7 %copy-start.7 = (bf16[1536,672]{0,1:T(8,128)(2,1)S(1)}, bf16[1536,672]{0,1:T(8,128)(2,1)}, u32[]{:S(2)}) copy-start(bf16[1536,672]{0,1:T(8,128)(2,1)} %copy-done.6) | copy-start | bytes 6193156
  126.9 17.4 %copy-start.2 = (bf16[384,256]{1,0:T(8,128)(2,1)S(1)}, bf16[384,256]{1,0:T(8,128)(2,1)}, u32[]{:S(2)}) copy-start(bf16[384,256]{1,0:T(8,128)(2,1)} %x_ref.1) | copy-start | bytes 589828
  126.9 59.2 %copy-start.4 = (bf16[384,256]{1,0:T(8,128)(2,1)S(1)}, bf16[384,256]{1,0:T(8,128)(2,1)}, u32[]{:S(2)}) copy-start(bf16[384,256]{1,0:T(8,128)(2,1)} %dy_ref.1) | copy-start | bytes 589828
Sparse Core Ops, SparseCore 0:
  105.9 38.3 reduce-scatter.1
